TPU v7x, 32 devices: a whole 2x2x4 slice. The times are simulated.
32 devices in a mesh: st: 16 (over z, y, x), tp: 2 (over core).
Axes of the slice: x: 2, y: 2, z: 4, core: 2. Of those that a mesh axis runs over, the one named last changes fastest.
Arguments:
- hidden: bfloat16 [8192, 2048], P('st'), may hold values from -24 to 24
- passage_store: bfloat16 [512, 64, 2048], P('st'), may hold values from -6 to 6
- passage_ids: int32 [128, 4], P('st'), may hold values from 0 to 511, as said below
- query_weight: bfloat16 [2048, 512], P(None, 'tp'), may hold values from -0.125 to 0.125
- gate_weight: bfloat16 [2048, 512], P(None, 'tp'), may hold values from -0.125 to 0.125
- key_weight: bfloat16 [2048, 512], P(None, 'tp'), may hold values from -0.125 to 0.125
- value_weight: bfloat16 [2048, 512], P(None, 'tp'), may hold values from -0.125 to 0.125
- output_grad: bfloat16 [8192, 512], P('st', 'tp'), may hold values from -6 to 6
Outputs:
- grad_hidden: bfloat16 [8192, 2048], P(('st', 'tp'))
- grad_store: bfloat16 [512, 64, 2048], P(('st', 'tp'))
- grad_value_weight: float32 [2048, 512], P(None, 'tp')
Inputs may be any that keep to these rules, and one draw needn't show every extreme that they name: `passage_ids`: passage p is held at st index p // 32. The 32 ids of one index of st (its 8 blocks) are distinct; at most 4 of them name passages of one owner, and on every index some owner is named exactly 4 times. Every index reads at least one passage of the owner before it, of the owner after it and of the owner half the axis away.
All inputs are finite; a program needn't handle non-finite values.
Results may differ from a plain program's by a relative error of at most 0.012.
The roundings to bfloat16 on the way count: a program that leaves them out, or rounds other values in their place, can miss the bound.
Values may be sent and summed in bfloat16 or wider, within the bound.
A program may use at most 128 MiB of HBM per device.

v0:
```python
import jax
import jax.numpy as jnp
from jax import lax
from jax.sharding import PartitionSpec as P

HEAD_DIM = 256


def body(
    hidden,
    passage_store,
    passage_ids,
    query_weight,
    gate_weight,
    key_weight,
    value_weight,
    output_grad,
):
    owner_count = lax.axis_size("st")
    own_index = lax.axis_index("st")
    held_count = passage_store.shape[0]
    span_rows = passage_store.shape[1]
    model_width = passage_store.shape[2]
    block_count = passage_ids.shape[0]
    per_block = passage_ids.shape[1]
    requests = block_count * per_block
    capacity = max(1, 2 * requests // owner_count)
    local_width = query_weight.shape[1]
    local_heads = local_width // HEAD_DIM
    tokens_here = hidden.shape[0]
    block_rows = tokens_here // block_count
    all_ids = lax.all_gather(passage_ids, "st", axis=0, tiled=True).reshape(owner_count, requests)
    owner_of = all_ids // held_count
    local_index = all_ids % held_count
    positions = jnp.arange(requests, dtype=jnp.int32)
    earlier = positions[None, :] < positions[:, None]
    matching = owner_of[:, :, None] == owner_of[:, None, :]
    slot_rank = jnp.sum(matching & earlier[None], axis=2)
    slot_iota = jnp.arange(capacity, dtype=jnp.int32)
    placed = (owner_of == own_index)[:, :, None] & (
        slot_rank[:, :, None] == slot_iota[None, None, :]
    )
    slot_table = jnp.sum(jnp.where(placed, local_index[:, :, None], 0), axis=1)
    filled = jnp.any(placed, axis=1)
    my_owner = lax.dynamic_index_in_dim(owner_of, own_index, 0, keepdims=False)
    my_rank = lax.dynamic_index_in_dim(slot_rank, own_index, 0, keepdims=False)
    slot_flat = my_owner * capacity + my_rank
    store_rows = passage_store.reshape(held_count * span_rows, model_width)
    keys_here = (
        jnp.dot(store_rows, key_weight, preferred_element_type=jnp.float32)
        .astype(jnp.bfloat16)
        .reshape(held_count, span_rows, local_width)
    )
    values_here = (
        jnp.dot(store_rows, value_weight, preferred_element_type=jnp.float32)
        .astype(jnp.bfloat16)
        .reshape(held_count, span_rows, local_width)
    )
    came_keys, came_values = (
        lax.all_to_all(keys_here[slot_table], "st", split_axis=0, concat_axis=0, tiled=True),
        lax.all_to_all(values_here[slot_table], "st", split_axis=0, concat_axis=0, tiled=True),
    )
    got_keys = came_keys.reshape(owner_count * capacity, span_rows, local_width)[slot_flat]
    got_values = came_values.reshape(owner_count * capacity, span_rows, local_width)[slot_flat]
    key_heads = got_keys.reshape(block_count, per_block * span_rows, local_heads, HEAD_DIM)
    value_heads = got_values.reshape(block_count, per_block * span_rows, local_heads, HEAD_DIM)
    queries = jnp.dot(hidden, query_weight, preferred_element_type=jnp.float32).astype(jnp.bfloat16)
    gates = jnp.dot(hidden, gate_weight, preferred_element_type=jnp.float32)
    query_heads = queries.reshape(block_count, block_rows, local_heads, HEAD_DIM)
    score_scale = HEAD_DIM ** (-0.5)
    scores = (
        jnp.einsum("bqhd,bkhd->bhqk", query_heads, key_heads, preferred_element_type=jnp.float32)
        * score_scale
    )
    probs = jax.nn.softmax(scores, axis=-1)
    probs_low = probs.astype(jnp.bfloat16)
    attended = jnp.einsum(
        "bhqk,bkhd->bqhd", probs_low, value_heads, preferred_element_type=jnp.float32
    ).reshape(tokens_here, local_width)
    gate_sigmoid = jax.nn.sigmoid(gates)
    upstream = output_grad.astype(jnp.float32)
    d_attended = (upstream * gates * gate_sigmoid).astype(jnp.bfloat16)
    d_gates = (upstream * attended * gate_sigmoid * (1.0 + gates * (1.0 - gate_sigmoid))).astype(
        jnp.bfloat16
    )
    d_heads = d_attended.reshape(block_count, block_rows, local_heads, HEAD_DIM)
    d_probs = jnp.einsum(
        "bqhd,bkhd->bhqk", d_heads, value_heads, preferred_element_type=jnp.float32
    )
    centre = jnp.sum(probs * d_probs, axis=-1, keepdims=True)
    d_scores = (probs * (d_probs - centre) * score_scale).astype(jnp.bfloat16)
    d_queries = (
        jnp.einsum("bhqk,bkhd->bqhd", d_scores, key_heads, preferred_element_type=jnp.float32)
        .astype(jnp.bfloat16)
        .reshape(tokens_here, local_width)
    )
    d_block_keys = jnp.einsum(
        "bhqk,bqhd->bkhd", d_scores, query_heads, preferred_element_type=jnp.float32
    ).reshape(requests, span_rows, local_width)
    d_block_values = jnp.einsum(
        "bhqk,bqhd->bkhd", probs_low, d_heads, preferred_element_type=jnp.float32
    ).reshape(requests, span_rows, local_width)
    contract = (((1,), (1,)), ((), ()))
    slot_total = owner_count * capacity
    back_keys = (
        jnp.zeros((slot_total, span_rows, local_width), jnp.float32).at[slot_flat].set(d_block_keys)
    )
    back_values = (
        jnp.zeros((slot_total, span_rows, local_width), jnp.float32)
        .at[slot_flat]
        .set(d_block_values)
    )
    came_dkeys, came_dvalues = (
        lax.all_to_all(
            back_keys.reshape(owner_count, capacity, span_rows, local_width),
            "st",
            split_axis=0,
            concat_axis=0,
            tiled=True,
        ),
        lax.all_to_all(
            back_values.reshape(owner_count, capacity, span_rows, local_width),
            "st",
            split_axis=0,
            concat_axis=0,
            tiled=True,
        ),
    )
    slot_owner = jnp.where(filled, slot_table, -1).reshape(slot_total)
    selector = (jnp.arange(held_count, dtype=jnp.int32)[:, None] == slot_owner[None, :]).astype(
        jnp.float32
    )
    key_totals = jnp.dot(
        selector,
        came_dkeys.reshape(slot_total, span_rows * local_width),
        precision=lax.Precision.HIGHEST,
        preferred_element_type=jnp.float32,
    )
    value_totals = jnp.dot(
        selector,
        came_dvalues.reshape(slot_total, span_rows * local_width),
        precision=lax.Precision.HIGHEST,
        preferred_element_type=jnp.float32,
    )
    key_low = key_totals.astype(jnp.bfloat16).reshape(held_count, span_rows, local_width)
    value_low = value_totals.astype(jnp.bfloat16).reshape(held_count, span_rows, local_width)
    weight_part = lax.dot_general(
        store_rows,
        value_low.reshape(held_count * span_rows, local_width),
        (((0,), (0,)), ((), ())),
        preferred_element_type=jnp.float32,
    )
    grad_value_weight = lax.psum(weight_part, "st")
    grad_hidden = lax.psum_scatter(
        lax.dot_general(d_queries, query_weight, contract, preferred_element_type=jnp.float32)
        + lax.dot_general(d_gates, gate_weight, contract, preferred_element_type=jnp.float32),
        "tp",
        scatter_dimension=0,
        tiled=True,
    ).astype(jnp.bfloat16)
    rows_key = key_low.reshape(
        held_count // lax.axis_size("tp") * lax.axis_size("tp") * span_rows, local_width
    )
    rows_value = value_low.reshape(
        held_count // lax.axis_size("tp") * lax.axis_size("tp") * span_rows, local_width
    )
    summed = lax.dot_general(
        rows_key, key_weight, contract, preferred_element_type=jnp.float32
    ) + lax.dot_general(rows_value, value_weight, contract, preferred_element_type=jnp.float32)
    grad_store = lax.psum_scatter(
        summed.reshape(
            held_count // lax.axis_size("tp") * lax.axis_size("tp"), span_rows, model_width
        ),
        "tp",
        scatter_dimension=0,
        tiled=True,
    ).astype(jnp.bfloat16)
    return (grad_hidden, grad_store, grad_value_weight)


def solution(mesh):
    placed = (
        P("st", None),
        P("st", None, None),
        P("st", None),
        P(None, "tp"),
        P(None, "tp"),
        P(None, "tp"),
        P(None, "tp"),
        P("st", "tp"),
    )
    return jax.shard_map(
        body,
        mesh=mesh,
        in_specs=placed,
        out_specs=(P(("st", "tp"), None), P(("st", "tp"), None, None), P(None, "tp")),
        check_vma=False,
    )
```

profile of v0, /device:TPU:0, one launch (start us, length us, event | category | flops | bytes accessed | tf_op | source)
XLA Modules:
  0.0 531.6 jit_solution(4978605036159977339)
XLA Ops:
  8.0 42.9 %all-gather = s32[16,8,4]{1,2,0:T(4,128)S(1)} all-gather(s32[1,8,4]{1,2,0:T(4,128)} %bitcast.110), channel_id=1, replica_groups=mesh['st'=16,'tp'=2] {'st'}, dimensions={0}, use_global_device_ids=true | all-gather | bytes 2176 | tf_op jit(solution)/shard_map/all_gather | solution.py:32
  52.0 6.0 %convolution_convert_fusion.2 = bf16[2048,256]{1,0:T(8,128)(2,1)S(1)} fusion(bf16[2048,2048]{1,0:T(8,128)(2,1)} %bitcast.89, bf16[2048,256]{1,0:T(8,128)(2,1)} %param.14), kind=kOutput, calls=%fused_computation.13 | convolution fusion | flops 2148007936 | bytes 10485760 | tf_op jit(solution)/shard_map/dot_general | solution.py:55
  60.0 4.4 all-to-all-start.1
  64.4 6.0 %convolution_convert_fusion.3 = bf16[2048,256]{1,0:T(8,128)(2,1)S(1)} fusion(bf16[2048,2048]{1,0:T(8,128)(2,1)} %bitcast.90, bf16[2048,256]{1,0:T(8,128)(2,1)} %param.13), kind=kOutput, calls=%fused_computation.14 | convolution fusion | flops 2148007936 | bytes 10485760 | tf_op jit(solution)/shard_map/dot_general | solution.py:50
  72.4 30.7 %all-to-all-done.1 = bf16[16,4,64,256]{3,2,1,0:T(8,128)(2,1)} async-done(((bf16[16,4,64,256]{3,2,1,0:T(8,128)(2,1)}), bf16[16,4,64,256]{3,2,1,0:T(8,128)(2,1)}, u32[]{:S(2)}, u32[]{:S(2)}) %all-to-all-start.1) | async-done | bytes 2097184 | tf_op jit(solution)/shard_map/all_to_all | solution.py:61
  103.1 7.6 %all-to-all-start = ((bf16[16,4,64,256]{3,2,1,0:T(8,128)(2,1)}), bf16[16,4,64,256]{3,2,1,0:T(8,128)(2,1)}, u32[]{:S(2)}, u32[]{:S(2)}) async-start(bf16[16,4,64,256]{3,2,1,0:T(8,128)(2,1)} %bitcast.95), calls=%async_computation | async-start | bytes 4194304 | tf_op jit(solution)/shard_map/all_to_all | solution.py:60
  111.4 3.3 gather_fusion.3
  114.7 36.4 %all-to-all-done = bf16[16,4,64,256]{3,2,1,0:T(8,128)(2,1)} async-done(((bf16[16,4,64,256]{3,2,1,0:T(8,128)(2,1)}), bf16[16,4,64,256]{3,2,1,0:T(8,128)(2,1)}, u32[]{:S(2)}, u32[]{:S(2)}) %all-to-all-start) | async-done | bytes 2097184 | tf_op jit(solution)/shard_map/all_to_all | solution.py:60
  155.5 3.3 fusion.22
  158.8 3.1 fusion.17
  163.1 4.9 fusion.8
  168.0 2.5 broadcast.191.clone
  170.6 5.3 %scatter_fusion = f32[64,64,256]{2,1,0:T(8,128)} fusion(f32[64,64,256]{2,1,0:T(8,128)} %broadcast.191.clone, s32[32]{0:T(128)S(1)} %fusion.30, f32[32,64,256]{2,1,0:T(8,128)S(1)} %bitcast.103), kind=kCustom, calls=%fused_computation.4 | custom fusion | bytes 6291584 | tf_op jit(solution)/shard_map/scatter | solution.py:106
  175.9 9.8 %all-to-all-start.2 = ((f32[16,4,64,256]{3,2,1,0:T(8,128)}), f32[16,4,64,256]{3,2,1,0:T(8,128)}, u32[]{:S(2)}, u32[]{:S(2)}) async-start(f32[16,4,64,256]{3,2,1,0:T(8,128)} %bitcast.88), calls=%async_computation.3 | async-start | bytes 8388608 | tf_op jit(solution)/shard_map/all_to_all | solution.py:114
  185.8 2.6 fusion.20
  188.3 2.5 broadcast.191.clone.1
  190.8 5.4 %scatter_fusion.1 = f32[64,64,256]{2,1,0:T(8,128)} fusion(f32[64,64,256]{2,1,0:T(8,128)} %broadcast.191.clone.1, s32[32]{0:T(128)S(1)} %fusion.30, f32[32,64,256]{2,1,0:T(8,128)S(1)} %bitcast.94), kind=kCustom, calls=%fused_computation.5 | custom fusion | bytes 6291584 | tf_op jit(solution)/shard_map/scatter | solution.py:111
  196.2 4.2 convolution_convert_fusion.4
  200.4 63.6 %all-to-all-done.2 = f32[16,4,64,256]{3,2,1,0:T(8,128)} async-done(((f32[16,4,64,256]{3,2,1,0:T(8,128)}), f32[16,4,64,256]{3,2,1,0:T(8,128)}, u32[]{:S(2)}, u32[]{:S(2)}) %all-to-all-start.2) | async-done | bytes 4194336 | tf_op jit(solution)/shard_map/all_to_all | solution.py:114
  264.0 19.2 %all-to-all-start.3 = ((f32[16,4,64,256]{3,2,1,0:T(8,128)}), f32[16,4,64,256]{3,2,1,0:T(8,128)}, u32[]{:S(2)}, u32[]{:S(2)}) async-start(f32[16,4,64,256]{3,2,1,0:T(8,128)} %bitcast.87), calls=%async_computation.4 | async-start | bytes 8388608 | tf_op jit(solution)/shard_map/all_to_all | solution.py:121
  284.5 2.8 convolution_add_fusion.1
  287.7 6.5 %copy.49 = f32[8,8,64,256]{3,1,2,0:T(8,128)} copy(f32[8,8,64,256]{3,2,1,0:T(8,128)} %bitcast.42) | data formatting | bytes 8388608
  294.3 67.3 %all-to-all-done.3 = f32[16,4,64,256]{3,2,1,0:T(8,128)} async-done(((f32[16,4,64,256]{3,2,1,0:T(8,128)}), f32[16,4,64,256]{3,2,1,0:T(8,128)}, u32[]{:S(2)}, u32[]{:S(2)}) %all-to-all-start.3) | async-done | bytes 4194336 | tf_op jit(solution)/shard_map/all_to_all | solution.py:121
  361.6 4.6 copy.50
  368.3 7.0 %convolution_bitcast_fusion = f32[2048,256]{0,1:T(8,128)} fusion(bf16[2048,256]{1,0:T(8,128)(2,1)S(1)} %reshape_reshape.8, bf16[2048,2048]{1,0:T(8,128)(2,1)} %bitcast.91), kind=kOutput, calls=%fused_computation.12 | convolution fusion | flops 2147483648 | bytes 11534336 | tf_op jit(solution)/shard_map/dot_general | solution.py:147
  375.6 3.8 convolution_convert_fusion.1
  380.0 3.6 fusion.38
  383.6 9.7 %convolution_add_fusion = f32[2048,2048]{1,0:T(8,128)} fusion(f32[2048,2048]{1,0:T(8,128)S(1)} %fusion.38, bf16[2048,256]{1,0:T(8,128)(2,1)S(1)} %reshape_reshape.8, bf16[2048,256]{1,0:T(8,128)(2,1)} %param.14), kind=kOutput, calls=%fused_computation.10 | convolution fusion | flops 2151677952 | bytes 35651584 | tf_op jit(solution)/shard_map/dot_general | solution.py:169
  393.4 3.0 convert_element_type.63
  396.4 118.7 %all-reduce.2.cloned.1.call-done = f32[2048,256]{0,1:T(8,128)} async-done(((f32[2048,256]{0,1:T(8,128)}), f32[2048,256]{0,1:T(8,128)}) %all-reduce.2.cloned.1.call-update) | async-done | bytes 2097168 | tf_op jit(solution)/shard_map/psum | solution.py:153
  515.1 3.0 copy.48
  518.1 6.0 %convert_element_type.66 = bf16[16,64,2048]{2,1,0:T(8,128)(2,1)} convert(f32[16,64,2048]{2,1,0:T(8,128)} %reduce-scatter.5.cloned.1.call-done) | non-fusion elementwise | flops 2097152 | bytes 12582912 | tf_op jit(solution)/shard_map/convert_element_type | solution.py:177
  (54 shorter events, 16.0 us)
Async XLA Ops:
  8.0 102.7 %copy-start = (bf16[512,2048]{1,0:T(8,128)(2,1)S(1)}, bf16[512,2048]{1,0:T(8,128)(2,1)}, u32[]{:S(2)}) copy-start(bf16[512,2048]{1,0:T(8,128)(2,1)} %param.8) | copy-start | bytes 6291460
  60.0 43.1 %all-to-all-start.1 = ((bf16[16,4,64,256]{3,2,1,0:T(8,128)(2,1)}), bf16[16,4,64,256]{3,2,1,0:T(8,128)(2,1)}, u32[]{:S(2)}, u32[]{:S(2)}) async-start(bf16[16,4,64,256]{3,2,1,0:T(8,128)(2,1)} %bitcast.96), calls=%async_computation.1 | async-start | bytes 4194304 | tf_op jit(solution)/shard_map/all_to_all | solution.py:61
  72.4 38.3 %copy-start.5 = (bf16[2048,256]{1,0:T(8,128)(2,1)S(1)}, bf16[2048,256]{1,0:T(8,128)(2,1)}, u32[]{:S(2)}) copy-start(bf16[2048,256]{1,0:T(8,128)(2,1)} %param.11) | copy-start | bytes 3145732
  103.1 48.0 %all-to-all-start = ((bf16[16,4,64,256]{3,2,1,0:T(8,128)(2,1)}), bf16[16,4,64,256]{3,2,1,0:T(8,128)(2,1)}, u32[]{:S(2)}, u32[]{:S(2)}) async-start(bf16[16,4,64,256]{3,2,1,0:T(8,128)(2,1)} %bitcast.95), calls=%async_computation | async-start | bytes 4194304 | tf_op jit(solution)/shard_map/all_to_all | solution.py:60
  111.4 44.1 %copy-start.8 = (bf16[512,256]{1,0:T(8,128)(2,1)}, bf16[512,256]{1,0:T(8,128)(2,1)S(1)}, u32[]{:S(2)}) copy-start(bf16[512,256]{1,0:T(8,128)(2,1)S(1)} %convolution_convert_fusion.5) | copy-start | bytes 786436
  153.7 0.8 copy-start.3
  158.8 3.1 copy-start.2
  175.9 88.1 %all-to-all-start.2 = ((f32[16,4,64,256]{3,2,1,0:T(8,128)}), f32[16,4,64,256]{3,2,1,0:T(8,128)}, u32[]{:S(2)}, u32[]{:S(2)}) async-start(f32[16,4,64,256]{3,2,1,0:T(8,128)} %bitcast.88), calls=%async_computation.3 | async-start | bytes 8388608 | tf_op jit(solution)/shard_map/all_to_all | solution.py:114
  264.0 19.3 %copy-start.6 = (bf16[2048,256]{1,0:T(8,128)(2,1)S(1)}, bf16[2048,256]{1,0:T(8,128)(2,1)}, u32[]{:S(2)}) copy-start(bf16[2048,256]{1,0:T(8,128)(2,1)} %param.11) | copy-start | bytes 3145732
  264.0 97.6 %all-to-all-start.3 = ((f32[16,4,64,256]{3,2,1,0:T(8,128)}), f32[16,4,64,256]{3,2,1,0:T(8,128)}, u32[]{:S(2)}, u32[]{:S(2)}) async-start(f32[16,4,64,256]{3,2,1,0:T(8,128)} %bitcast.87), calls=%async_computation.4 | async-start | bytes 8388608 | tf_op jit(solution)/shard_map/all_to_all | solution.py:121
  283.2 1.2 copy-start.4
  283.2 1.3 copy-start.7
  283.2 110.1 %reduce-scatter.3.cloned.1.call-start = ((), (), s32[]{:S(2)}) async-start(), calls=%async_computation.6 | async-start | bytes 6291456 | tf_op jit(solution)/shard_map/reduce_scatter | solution.py:154
  287.4 227.7 %all-reduce.2.cloned.1.call-start = ((), (), s32[]{:S(2)}) async-start(), calls=%async_computation.8 | async-start | bytes 4194304 | tf_op jit(solution)/shard_map/psum | solution.py:153
  375.4 142.7 %reduce-scatter.5.cloned.1.call-start = ((), (), s32[]{:S(2)}) async-start(), calls=%async_computation.7 | async-start | bytes 25165824 | tf_op jit(solution)/shard_map/reduce_scatter | solution.py:170
  515.1 9.1 %copy-start.1 = (bf16[512,2048]{1,0:T(8,128)(2,1)S(1)}, bf16[512,2048]{1,0:T(8,128)(2,1)}, u32[]{:S(2)}) copy-start(bf16[512,2048]{1,0:T(8,128)(2,1)} %param.8) | copy-start | bytes 6291460
Sparse Core Ops, SparseCore 0:
  287.5 13.2 reduce-scatter.2
  393.5 38.9 reduce-scatter.4
Sparse Core Ops, SparseCore 1:
  375.5 139.5 all-reduce.1
where the time goes:
time: 533 us; the launch traced here: 532 us
  waiting for transfers between devices  317 us (59%)
  matrix products  61.7 us (12%)
  blocking collectives  42.9 us (8%)
  local copies, waits for them, and re-layouts  42.2 us (8%)
  starting transfers between devices  41.4 us (8%)
  between operations  15.7 us (3%)
  other arithmetic  10.9 us (2%)
    psum x1, waiting for transfers between devices, body(): grad_value_weight = lax.psum(weight_part, 'st')  119 us
    all_to_all x1, waiting for transfers between devices, body(): lax.all_to_all(back_values.reshape(owner_count, capacity, span_rows, loca...  67.3 us
    all_to_all x1, waiting for transfers between devices, body(): lax.all_to_all(back_keys.reshape(owner_count, capacity, span_rows, local_...  63.6 us
    all_gather x1, blocking collectives, body(): lax.all_gather(passage_ids, 'st', axis=0, tiled=True)  42.9 us
    all_to_all x1, waiting for transfers between devices, body(): lax.all_to_all(keys_here[slot_table], 'st', split_axis=0, concat_axis=0,...  36.4 us
    all_to_all x1, waiting for transfers between devices, body(): lax.all_to_all(values_here[slot_table], 'st', split_axis=0, concat_axis=0...  30.7 us
    all_to_all x1, starting transfers between devices, body(): lax.all_to_all(back_values.reshape(owner_count, capacity, span_rows, loca...  19.2 us
    unnamed x21, local copies, waits for them, and re-layouts  15.4 us
  transfers between devices with their start and end apart: 7, of which 5 were waited for; matrix products, arithmetic and copies ran while one was open for 14% of the time, Pallas kernels for 0%

commit v1 on v0

--- a/solution.py
+++ b/solution.py
@@ -150,7 +150,11 @@
         (((0,), (0,)), ((), ())),
         preferred_element_type=jnp.float32,
     )
-    grad_value_weight = lax.psum(weight_part, "st")
+    grad_value_weight = weight_part
+    for hop in (1, 2, 4, 8):
+        grad_value_weight = grad_value_weight + lax.ppermute(
+            grad_value_weight, "st", [(dev, dev ^ hop) for dev in range(16)]
+        )
     grad_hidden = lax.psum_scatter(
         lax.dot_general(d_queries, query_weight, contract, preferred_element_type=jnp.float32)
         + lax.dot_general(d_gates, gate_weight, contract, preferred_element_type=jnp.float32),

time: 533 us -> 651 us (1.22)
  waiting for transfers between devices: 317 us -> 417 us
  starting transfers between devices: 41.4 us -> 62.5 us
    ppermute x0 -> x4, waiting for transfers between devices: none -> 219 us  [body(): lax.ppermute(grad_value_weight, 'st', [(dev, dev ^ hop) for dev in range(...]
    psum x1 -> x0, waiting for transfers between devices: 119 us -> none  [body(): grad_value_weight = lax.psum(weight_part, 'st')]
    ppermute x0 -> x4, starting transfers between devices: none -> 21.3 us  [body(): lax.ppermute(grad_value_weight, 'st', [(dev, dev ^ hop) for dev in range(...]
  transfers between devices with their start and end apart: 7 -> 10, of which waited for: 5 -> 8; matrix products, arithmetic and copies ran while one was open for 14% -> 11% of each run, Pallas kernels for 0% -> 0%
where the time goes in v1:
time: 651 us; the launch traced here: 650 us
  waiting for transfers between devices  417 us (64%)
  starting transfers between devices  62.5 us (10%)
  matrix products  58.2 us (9%)
  blocking collectives  42.9 us (7%)
  local copies, waits for them, and re-layouts  40.3 us (6%)
  other arithmetic  14.7 us (2%)
  between operations  14.3 us (2%)
    ppermute x4, waiting for transfers between devices, body(): lax.ppermute(grad_value_weight, 'st', [(dev, dev ^ hop) for dev in range(...  219 us
    all_to_all x1, waiting for transfers between devices, body(): lax.all_to_all(back_keys.reshape(owner_count, capacity, span_rows, local_...  67.8 us
    all_to_all x1, waiting for transfers between devices, body(): lax.all_to_all(back_values.reshape(owner_count, capacity, span_rows, loca...  62.9 us
    all_gather x1, blocking collectives, body(): lax.all_gather(passage_ids, 'st', axis=0, tiled=True)  42.9 us
    all_to_all x1, waiting for transfers between devices, body(): lax.all_to_all(keys_here[slot_table], 'st', split_axis=0, concat_axis=0,...  36.4 us
    all_to_all x1, waiting for transfers between devices, body(): lax.all_to_all(values_here[slot_table], 'st', split_axis=0, concat_axis=0...  30.7 us
    ppermute x4, starting transfers between devices, body(): lax.ppermute(grad_value_weight, 'st', [(dev, dev ^ hop) for dev in range(...  21.3 us
    all_to_all x1, starting transfers between devices, body(): lax.all_to_all(back_values.reshape(owner_count, capacity, span_rows, loca...  19.1 us
  transfers between devices with their start and end apart: 10, of which 8 were waited for; matrix products, arithmetic and copies ran while one was open for 11% of the time, Pallas kernels for 0%

profile of v1, /device:TPU:0, one launch (start us, length us, event | category | flops | bytes accessed | tf_op | source)
XLA Modules:
  0.0 649.9 jit_solution(15690118481992731476)
XLA Ops:
  7.2 42.9 %all-gather = s32[16,8,4]{1,2,0:T(4,128)S(1)} all-gather(s32[1,8,4]{1,2,0:T(4,128)} %bitcast.110), channel_id=1, replica_groups=mesh['st'=16,'tp'=2] {'st'}, dimensions={0}, use_global_device_ids=true | all-gather | bytes 2176 | tf_op jit(solution)/shard_map/all_gather | solution.py:32
  51.2 6.0 convolution_convert_fusion.2
  59.1 4.4 all-to-all-start.1
  63.6 6.0 convolution_convert_fusion.3
  71.5 30.7 %all-to-all-done.1 = bf16[16,4,64,256]{3,2,1,0:T(8,128)(2,1)} async-done(((bf16[16,4,64,256]{3,2,1,0:T(8,128)(2,1)}), bf16[16,4,64,256]{3,2,1,0:T(8,128)(2,1)}, u32[]{:S(2)}, u32[]{:S(2)}) %all-to-all-start.1) | async-done | bytes 2097184 | tf_op jit(solution)/shard_map/all_to_all | solution.py:61
  102.2 7.7 %all-to-all-start = ((bf16[16,4,64,256]{3,2,1,0:T(8,128)(2,1)}), bf16[16,4,64,256]{3,2,1,0:T(8,128)(2,1)}, u32[]{:S(2)}, u32[]{:S(2)}) async-start(bf16[16,4,64,256]{3,2,1,0:T(8,128)(2,1)} %bitcast.95), calls=%async_computation | async-start | bytes 4194304 | tf_op jit(solution)/shard_map/all_to_all | solution.py:60
  110.7 3.3 gather_fusion.3
  114.0 36.4 %all-to-all-done = bf16[16,4,64,256]{3,2,1,0:T(8,128)(2,1)} async-done(((bf16[16,4,64,256]{3,2,1,0:T(8,128)(2,1)}), bf16[16,4,64,256]{3,2,1,0:T(8,128)(2,1)}, u32[]{:S(2)}, u32[]{:S(2)}) %all-to-all-start) | async-done | bytes 2097184 | tf_op jit(solution)/shard_map/all_to_all | solution.py:60
  154.8 3.3 fusion.22
  158.1 3.1 fusion.17
  162.4 4.9 fusion.8
  169.9 5.3 scatter_fusion
  175.2 9.9 %all-to-all-start.2 = ((f32[16,4,64,256]{3,2,1,0:T(8,128)}), f32[16,4,64,256]{3,2,1,0:T(8,128)}, u32[]{:S(2)}, u32[]{:S(2)}) async-start(f32[16,4,64,256]{3,2,1,0:T(8,128)} %bitcast.88), calls=%async_computation.3 | async-start | bytes 8388608 | tf_op jit(solution)/shard_map/all_to_all | solution.py:114
  190.1 5.4 scatter_fusion.1
  195.5 67.8 %all-to-all-done.2 = f32[16,4,64,256]{3,2,1,0:T(8,128)} async-done(((f32[16,4,64,256]{3,2,1,0:T(8,128)}), f32[16,4,64,256]{3,2,1,0:T(8,128)}, u32[]{:S(2)}, u32[]{:S(2)}) %all-to-all-start.2) | async-done | bytes 4194336 | tf_op jit(solution)/shard_map/all_to_all | solution.py:114
  263.3 19.1 %all-to-all-start.3 = ((f32[16,4,64,256]{3,2,1,0:T(8,128)}), f32[16,4,64,256]{3,2,1,0:T(8,128)}, u32[]{:S(2)}, u32[]{:S(2)}) async-start(f32[16,4,64,256]{3,2,1,0:T(8,128)} %bitcast.87), calls=%async_computation.4 | async-start | bytes 8388608 | tf_op jit(solution)/shard_map/all_to_all | solution.py:121
  282.4 4.2 convolution_convert_fusion.4
  291.1 4.6 copy.49
  297.9 62.9 %all-to-all-done.3 = f32[16,4,64,256]{3,2,1,0:T(8,128)} async-done(((f32[16,4,64,256]{3,2,1,0:T(8,128)}), f32[16,4,64,256]{3,2,1,0:T(8,128)}, u32[]{:S(2)}, u32[]{:S(2)}) %all-to-all-start.3) | async-done | bytes 4194336 | tf_op jit(solution)/shard_map/all_to_all | solution.py:121
  360.7 4.6 copy.50
  367.7 3.6 fusion.38
  371.3 9.7 %convolution_add_fusion = f32[2048,2048]{1,0:T(8,128)} fusion(f32[2048,2048]{1,0:T(8,128)S(1)} %fusion.38, bf16[2048,256]{1,0:T(8,128)(2,1)S(1)} %reshape_reshape.8, bf16[2048,256]{1,0:T(8,128)(2,1)} %param.14), kind=kOutput, calls=%fused_computation.10 | convolution fusion | flops 2151677952 | bytes 35651584 | tf_op jit(solution)/shard_map/dot_general | solution.py:173
  381.0 5.7 convolution_bitcast_fusion
  388.9 43.9 %collective-permute-done = f32[2048,256]{0,1:T(8,128)S(1)} collective-permute-done((f32[2048,256]{0,1:T(8,128)S(1)}, f32[2048,256]{0,1:T(8,128)S(1)}, u32[]{:S(2)}, u32[]{:S(2)}) %collective-permute-start) | collective-permute-done | bytes 2097184 | tf_op jit(solution)/shard_map/ppermute | solution.py:155
  433.0 6.2 collective-permute-start.1
  439.3 43.3 %collective-permute-done.1 = f32[2048,256]{0,1:T(8,128)S(1)} collective-permute-done((f32[2048,256]{0,1:T(8,128)S(1)}, f32[2048,256]{0,1:T(8,128)S(1)}, u32[]{:S(2)}, u32[]{:S(2)}) %collective-permute-start.1) | collective-permute-done | bytes 2097184 | tf_op jit(solution)/shard_map/ppermute | solution.py:155
  482.9 12.9 %collective-permute-start.2 = (f32[2048,256]{0,1:T(8,128)S(1)}, f32[2048,256]{0,1:T(8,128)S(1)}, u32[]{:S(2)}, u32[]{:S(2)}) collective-permute-start(f32[2048,256]{0,1:T(8,128)S(1)} %add.103), channel_id=1, source_target_pairs={{0,8},{2,10},{4,12},{6,14},{8,0},{10,2},{12,4},{14,6},{16,24},{18,... | collective-permute-start | bytes 6291464 | tf_op jit(solution)/shard_map/ppermute | solution.py:155
  495.8 44.2 %collective-permute-done.2 = f32[2048,256]{0,1:T(8,128)S(1)} collective-permute-done((f32[2048,256]{0,1:T(8,128)S(1)}, f32[2048,256]{0,1:T(8,128)S(1)}, u32[]{:S(2)}, u32[]{:S(2)}) %collective-permute-start.2) | collective-permute-done | bytes 2097184 | tf_op jit(solution)/shard_map/ppermute | solution.py:155
  543.0 87.7 %collective-permute-done.3 = f32[2048,256]{0,1:T(8,128)} collective-permute-done((f32[2048,256]{0,1:T(8,128)S(1)}, f32[2048,256]{0,1:T(8,128)}, u32[]{:S(2)}, u32[]{:S(2)}) %collective-permute-start.3) | collective-permute-done | bytes 2097184 | tf_op jit(solution)/shard_map/ppermute | solution.py:155
  630.7 3.2 add.105
  634.0 2.9 copy.48
  636.9 6.2 convert_element_type.66
  (63 shorter events, 33.7 us)
Async XLA Ops:
  7.2 102.8 %copy-start = (bf16[512,2048]{1,0:T(8,128)(2,1)S(1)}, bf16[512,2048]{1,0:T(8,128)(2,1)}, u32[]{:S(2)}) copy-start(bf16[512,2048]{1,0:T(8,128)(2,1)} %param.8) | copy-start | bytes 6291460
  59.1 43.1 %all-to-all-start.1 = ((bf16[16,4,64,256]{3,2,1,0:T(8,128)(2,1)}), bf16[16,4,64,256]{3,2,1,0:T(8,128)(2,1)}, u32[]{:S(2)}, u32[]{:S(2)}) async-start(bf16[16,4,64,256]{3,2,1,0:T(8,128)(2,1)} %bitcast.96), calls=%async_computation.1 | async-start | bytes 4194304 | tf_op jit(solution)/shard_map/all_to_all | solution.py:61
  102.2 7.8 %copy-start.5 = (bf16[2048,256]{1,0:T(8,128)(2,1)S(1)}, bf16[2048,256]{1,0:T(8,128)(2,1)}, u32[]{:S(2)}) copy-start(bf16[2048,256]{1,0:T(8,128)(2,1)} %param.11) | copy-start | bytes 3145732
  102.2 48.2 %all-to-all-start = ((bf16[16,4,64,256]{3,2,1,0:T(8,128)(2,1)}), bf16[16,4,64,256]{3,2,1,0:T(8,128)(2,1)}, u32[]{:S(2)}, u32[]{:S(2)}) async-start(bf16[16,4,64,256]{3,2,1,0:T(8,128)(2,1)} %bitcast.95), calls=%async_computation | async-start | bytes 4194304 | tf_op jit(solution)/shard_map/all_to_all | solution.py:60
  110.7 41.9 %copy-start.8 = (bf16[512,256]{1,0:T(8,128)(2,1)}, bf16[512,256]{1,0:T(8,128)(2,1)S(1)}, u32[]{:S(2)}) copy-start(bf16[512,256]{1,0:T(8,128)(2,1)S(1)} %convolution_convert_fusion.5) | copy-start | bytes 786436
  153.1 0.8 copy-start.3
  158.1 3.1 copy-start.2
  175.2 88.1 %all-to-all-start.2 = ((f32[16,4,64,256]{3,2,1,0:T(8,128)}), f32[16,4,64,256]{3,2,1,0:T(8,128)}, u32[]{:S(2)}, u32[]{:S(2)}) async-start(f32[16,4,64,256]{3,2,1,0:T(8,128)} %bitcast.88), calls=%async_computation.3 | async-start | bytes 8388608 | tf_op jit(solution)/shard_map/all_to_all | solution.py:114
  263.3 97.4 %all-to-all-start.3 = ((f32[16,4,64,256]{3,2,1,0:T(8,128)}), f32[16,4,64,256]{3,2,1,0:T(8,128)}, u32[]{:S(2)}, u32[]{:S(2)}) async-start(f32[16,4,64,256]{3,2,1,0:T(8,128)} %bitcast.87), calls=%async_computation.4 | async-start | bytes 8388608 | tf_op jit(solution)/shard_map/all_to_all | solution.py:121
  282.4 4.3 copy-start.6
  282.4 257.9 %reduce-scatter.3.cloned.1.call-start = ((), (), s32[]{:S(2)}) async-start(), calls=%async_computation.6 | async-start | bytes 6291456 | tf_op jit(solution)/shard_map/reduce_scatter | solution.py:158
  286.7 1.2 copy-start.4
  286.7 1.3 copy-start.7
  290.7 346.1 %reduce-scatter.5.cloned.1.call-start = ((), (), s32[]{:S(2)}) async-start(), calls=%async_computation.7 | async-start | bytes 25165824 | tf_op jit(solution)/shard_map/reduce_scatter | solution.py:174
  386.8 46.0 %collective-permute-start = (f32[2048,256]{0,1:T(8,128)S(1)}, f32[2048,256]{0,1:T(8,128)S(1)}, u32[]{:S(2)}, u32[]{:S(2)}) collective-permute-start(f32[2048,256]{0,1:T(8,128)S(1)} %convolution_bitcast_fusion), channel_id=1, source_target_pairs={{0,2},{2,0},{4,6},{6,4},{8,10},{10,8},{12,14},{14,12},{16,18},{18,... | collective-permute-start | bytes 6291464 | tf_op jit(solution)/shard_map/ppermute | solution.py:155
  433.0 49.6 %collective-permute-start.1 = (f32[2048,256]{0,1:T(8,128)S(1)}, f32[2048,256]{0,1:T(8,128)S(1)}, u32[]{:S(2)}, u32[]{:S(2)}) collective-permute-start(f32[2048,256]{0,1:T(8,128)S(1)} %add.102), channel_id=1, source_target_pairs={{0,4},{2,6},{4,0},{6,2},{8,12},{10,14},{12,8},{14,10},{16,20},{18,... | collective-permute-start | bytes 6291464 | tf_op jit(solution)/shard_map/ppermute | solution.py:155
  482.9 57.0 %collective-permute-start.2 = (f32[2048,256]{0,1:T(8,128)S(1)}, f32[2048,256]{0,1:T(8,128)S(1)}, u32[]{:S(2)}, u32[]{:S(2)}) collective-permute-start(f32[2048,256]{0,1:T(8,128)S(1)} %add.103), channel_id=1, source_target_pairs={{0,8},{2,10},{4,12},{6,14},{8,0},{10,2},{12,4},{14,6},{16,24},{18,... | collective-permute-start | bytes 6291464 | tf_op jit(solution)/shard_map/ppermute | solution.py:155
  540.2 90.5 %collective-permute-start.3 = (f32[2048,256]{0,1:T(8,128)S(1)}, f32[2048,256]{0,1:T(8,128)}, u32[]{:S(2)}, u32[]{:S(2)}) collective-permute-start(f32[2048,256]{0,1:T(8,128)S(1)} %add.104), channel_id=1, source_target_pairs={{0,16},{2,18},{4,20},{6,22},{8,24},{10,26},{12,28},{14,30},{16,0},... | collective-permute-start | bytes 6291464 | tf_op jit(solution)/shard_map/ppermute | solution.py:155
  636.9 6.2 copy-start.1
Sparse Core Ops, SparseCore 0:
  290.8 13.2 reduce-scatter.2
  381.2 38.7 reduce-scatter.4
